TPU v7x, 32 devices: a whole 2x2x4 slice. The times are simulated.
32 devices in a mesh: sp: 8 (over z, y), tp: 4 (over x, core).
Axes of the slice: x: 2, y: 2, z: 4, core: 2. Of those that a mesh axis runs over, the one named last changes fastest.
Arguments:
- queries: bfloat16 [4096, 1024], P('sp', 'tp'), may hold values from -6 to 6
- keys: bfloat16 [4096, 1024], P('sp', 'tp'), may hold values from -6 to 6
- values: bfloat16 [4096, 1024], P('sp', 'tp'), may hold values from -6 to 6
- cum_gate: float32 [4096, 16], P('sp', 'tp'), as said below
- documents: int32 [4096], P('sp'), may hold values from 0 to 3, never falling along the last dimension, each value on 1 to 2048 neighbouring positions
- head_gain: float32 [1024], P('tp'), may hold values from 0.1 to 1.9
- out_weight: bfloat16 [1024, 2048], replicated, may hold values from -0.1875 to 0.1875
- resid: bfloat16 [4096, 2048], P(('sp', 'tp')), may hold values from -6 to 6
- norm_gain: float32 [2048], replicated, may hold values from 0.1 to 1.9
- routes: int32 [4096, 2], P(('sp', 'tp')), may hold values from 0 to 7, all different within a row; in each aligned block of 128 rows (0 to 127, 128 to 255, ...) at most 64 rows name the same one
- route_weights: float32 [4096, 2], P(('sp', 'tp')), may hold values from 0.25 to 1
- w_gate: bfloat16 [8, 2048, 3584], P('sp', None, 'tp'), may hold values from -0.125 to 0.125
- w_up: bfloat16 [8, 2048, 3584], P('sp', None, 'tp'), may hold values from -0.125 to 0.125
- w_down: bfloat16 [8, 3584, 2048], P('sp', 'tp'), may hold values from -0.09375 to 0.09375
Outputs:
- mixed: bfloat16 [4096, 2048], P(('sp', 'tp'))
Inputs may be any that keep to these rules, and one draw needn't show every extreme that they name: `cum_gate`: along the positions each head's values never rise. `documents`: document numbers never fall along the positions. `routes`: the 2 experts of a row differ. In each aligned block of 128 rows no expert is named more than 64 times; in some blocks an expert is named exactly 64 times.
All inputs are finite; a program needn't handle non-finite values.
Results may differ from a plain program's by a relative error of at most 0.015.
Values may be sent and summed in bfloat16 or wider, within the bound.
A program may use at most 128 MiB of HBM per device.

v0:
```python
import functools

import jax
import jax.numpy as jnp
from jax import lax
from jax.experimental import pallas as pl
from jax.experimental.pallas import tpu as pltpu
from jax.sharding import PartitionSpec as P

EPS = 1e-06
MESH = pl.DeviceIdType.MESH
NEG = -1e30
VMEM_LIMIT = 65000 * 1024
LANES = 128
SPLITS = 2
BF = jnp.bfloat16
F32 = jnp.float32


def layer_kernel(
    n,
    head_size,
    cap,
    q_hbm,
    k_hbm,
    v_hbm,
    aux_ref,
    gain_ref,
    wo_hbm,
    resid_hbm,
    norm_gain_ref,
    routes_ref,
    routes_t_ref,
    route_w_ref,
    wg_hbm,
    wu_hbm,
    wd_hbm,
    mixed_ref,
    q_in,
    qs,
    kv,
    aux_all,
    top,
    acc,
    normed,
    gathered,
    wo,
    resid,
    wide,
    xin,
    into,
    out_ref,
    ret_ref,
    fan,
    wg,
    wu,
    wd,
    hidden,
    part,
    got,
    pair,
    across,
    fin,
    in_sem,
    kv_sem,
    w_sem,
    own_sem,
    up_send,
    up_recv,
    over_send,
    over_recv,
    aux_send,
    aux_recv,
    h_send,
    h_recv,
    a_send,
    a_recv,
    x_send,
    x_recv,
    c_send,
    c_recv,
    d_send,
    d_recv,
    p_send,
    p_recv,
    s_send,
    s_recv,
    r_send,
    r_recv,
):
    me = lax.axis_index("sp")
    t = lax.axis_index("tp")
    c, xi = lax.rem(t, 2), t // 2
    near = xi * 2 + (1 - c)
    far = (1 - xi) * 2 + c
    diag = 3 - t
    y, z = lax.rem(me, 2), me // 2
    floors, reach = n // 2, n // 4
    near_id = {"sp": me, "tp": near}
    far_id = {"sp": me, "tp": far}
    diag_id = {"sp": me, "tp": diag}
    mate_id = {"sp": me + 1 - 2 * y, "tp": t}
    above_id = {"sp": lax.rem(me + 2, n), "tp": t}

    tokens, width_here = q_in.shape
    pairs = width_here // LANES
    hpp = LANES // head_size
    keys = tokens // SPLITS
    chunks = pairs * SPLITS
    rows, width = mixed_ref.shape

    loads = [
        pltpu.make_async_copy(
            src.at[pl.ds(s * keys, keys), pl.ds(p * LANES, LANES)],
            kv.at[0, p * SPLITS + s, j],
            kv_sem.at[(p * SPLITS + s) * 2 + j],
        )
        for p in range(pairs)
        for s in range(SPLITS)
        for j, src in enumerate((k_hbm, v_hbm))
    ]
    q_load = pltpu.make_async_copy(q_hbm, q_in, in_sem.at[0])
    wo_load = pltpu.make_async_copy(wo_hbm, wo, in_sem.at[1])
    resid_load = pltpu.make_async_copy(resid_hbm, resid, in_sem.at[2])
    weights = [
        pltpu.make_async_copy(src, dst, w_sem.at[i])
        for i, (src, dst) in enumerate(((wg_hbm, wg), (wu_hbm, wu), (wd_hbm, wd)))
    ]
    for copy in loads:
        copy.start()
    q_load.start()

    barrier = pltpu.get_barrier_semaphore()

    def greet(k, carry):
        pl.semaphore_signal(
            barrier,
            inc=1,
            device_id={"sp": lax.rem(me + k, n), "tp": t},
            device_id_type=MESH,
        )
        return carry

    lax.fori_loop(1, n, greet, 0)
    for other in (near_id, far_id, diag_id):
        pl.semaphore_signal(barrier, inc=1, device_id=other, device_id_type=MESH)

    def remote(src, dst, send, recv, to):
        return pltpu.make_async_remote_copy(
            src_ref=src, dst_ref=dst, send_sem=send, recv_sem=recv, device_id=to, device_id_type=MESH
        )

    def up(d, i):
        return remote(
            kv.at[d, i],
            kv.at[d + 1, i],
            up_send.at[d * chunks + i],
            up_recv.at[d * chunks + i],
            above_id,
        )

    def over(d, i):
        return remote(
            kv.at[d, i],
            kv.at[reach + 1 + d, i],
            over_send.at[d * chunks + i],
            over_recv.at[d * chunks + i],
            mate_id,
        )

    def aux_copy(k):
        return remote(
            aux_ref,
            aux_all.at[k],
            aux_send.at[k],
            aux_recv.at[k],
            {"sp": lax.rem(me + k, n), "tp": t},
        )

    def rising(d):
        return (z + 1 < floors) & (z >= d) & (d < reach)

    def crossing(d):
        return (z >= d) & ((d > 0) | (y == 0)) & ((d < reach) | (y == 1))

    def coming(d):
        return (z >= d) & ((d > 0) | (y == 1)) & ((d < reach) | (y == 0))

    def forward(d, i):
        @pl.when(rising(d))
        def _():
            up(d, i).start()

        @pl.when(crossing(d))
        def _():
            over(d, i).start()

    for copy in loads:
        copy.wait()
    pl.semaphore_wait(barrier, n + 2)
    lax.fori_loop(0, chunks, lambda i, z_: (forward(0, i), z_)[1], 0)

    def send_aux(k, carry):
        @pl.when(me + k < n)
        def _():
            aux_copy(k).start()

        return carry

    lax.fori_loop(1, n // 2 + 1, send_aux, 0)
    wo_load.start()
    resid_load.start()
    for copy in weights:
        copy.start()

    lane = lax.broadcasted_iota(jnp.int32, (1, LANES), 1)
    tile = min(tokens, 256)

    def mine(h):
        return (lane >= h * head_size) & (lane < (h + 1) * head_size)

    q_load.wait()
    for p in range(pairs):
        block = q_in[:, p * LANES : (p + 1) * LANES].astype(F32) * (head_size ** (-0.5))
        for h in range(hpp):
            qs[p, h] = jnp.where(mine(h), block, 0.0).astype(BF)
    top[...] = jnp.full(top.shape, NEG, F32)
    acc[...] = jnp.zeros(acc.shape, F32)

    def wider(x):
        return jnp.concatenate([x] * (keys // LANES), axis=1) if keys > LANES else x[:, :keys]

    def visit(slot, i, p, h, r0, bias, allowed):
        at = pl.ds(r0, tile)
        k = kv[slot, i, 0]
        v = jnp.where(mine(h), kv[slot, i, 1].astype(F32), 1.0).astype(BF)
        scores = lax.dot_general(
            qs[p, h, at, :], k, (((1,), (1,)), ((), ())), preferred_element_type=F32
        )
        scores = scores + bias
        if allowed is not None:
            scores = jnp.where(allowed, scores, NEG)
        before = top[p, h, at, :]
        highest = jnp.maximum(before, jnp.max(scores, axis=1, keepdims=True))
        exps = jnp.exp(scores - wider(highest))
        rescale = jnp.exp(before - highest)
        top[p, h, at, :] = highest
        acc[p, h, at, :] = acc[p, h, at, :] * rescale + jnp.dot(
            exps.astype(BF), v, preferred_element_type=F32
        )

    first_doc = aux_ref[0][hpp : hpp + 1, 0:1]
    spots_r = lax.broadcasted_iota(jnp.int32, (keys, keys), 0)
    spots_c = lax.broadcasted_iota(jnp.int32, (keys, keys), 1)
    doc_cols = [
        jnp.sum(
            jnp.where(spots_r == spots_c, aux_ref[s][hpp : hpp + 1, :], 0.0), axis=1, keepdims=True
        )
        for s in range(SPLITS)
    ]
    doc_col = jnp.concatenate(doc_cols, axis=0)

    def diagonal(p, carry):
        for s in range(SPLITS):
            i = p * SPLITS + s
            side = aux_ref[i]
            for h in range(hpp):
                base = aux_ref[p * SPLITS][h : h + 1, 0:1]
                bias = base - side[h : h + 1, :]
                for r0 in range(0, tokens, tile):
                    if r0 + tile <= s * keys:
                        continue
                    key_pos = s * keys + lax.broadcasted_iota(jnp.int32, (1, keys), 1)
                    query_pos = r0 + lax.broadcasted_iota(jnp.int32, (tile, 1), 0)
                    allowed = (key_pos <= query_pos) & (
                        side[hpp : hpp + 1, :] == doc_col[r0 : r0 + tile]
                    )
                    visit(0, i, p, h, r0, bias, allowed)
        return carry

    lax.fori_loop(0, pairs, diagonal, 0)
    shut = jnp.where(doc_col == first_doc, 0.0, 2e30)
    for p in range(pairs):
        for h in range(hpp):
            top[p, h] = jnp.where(shut > 0.0, 1e30, top[p, h])

    def earlier(slot, dist, i):
        p = i // SPLITS
        side = aux_all[dist, i]
        zero = aux_ref[p * SPLITS]
        for h in range(hpp):
            bias = jnp.where(
                side[hpp : hpp + 1, :] == first_doc, zero[h : h + 1, 0:1] - side[h : h + 1, :], NEG
            )
            for r0 in range(0, tokens, tile):
                visit(slot, i, p, h, r0, bias, None)

    def aux_here(k, i):
        @pl.when(i == 0)
        def _():
            aux_copy(k).wait_recv()

    def crossed(d, i):
        @pl.when(coming(d))
        def _():
            dist = 2 * d + 2 * y - 1
            aux_here(dist, i)
            over(d, i).wait_recv()
            earlier(reach + 1 + d, dist, i)

    def history(j, carry):
        d, i = j // chunks + 1, lax.rem(j, chunks)

        @pl.when(z >= d)
        def _():
            up(d - 1, i).wait_recv()
            forward(d, i)
            aux_here(2 * d, i)
            earlier(d, 2 * d, i)

        crossed(d - 1, i)
        return carry

    lax.fori_loop(0, reach * chunks, history, 0)
    lax.fori_loop(0, chunks, lambda i, z_: (crossed(reach, i), z_)[1], 0)

    def h_copy(q, to):
        return remote(normed.at[q], gathered.at[t], h_send.at[q], h_recv.at[t], to)

    def h_in(q):
        return remote(normed.at[q], gathered.at[q], h_send.at[q], h_recv.at[q], near_id)

    def settle(q):
        at = pl.ds(pl.multiple_of(q * rows, rows), rows)
        for p in range(pairs):
            total = None
            for h in range(hpp):
                state = acc[p, h, at, :]
                sums = pltpu.roll(state, head_size, 1)
                attended = jnp.where(mine(h), state / sums, 0.0)
                mean_square = jnp.sum(attended * attended, axis=1, keepdims=True) / head_size
                piece = attended * lax.rsqrt(mean_square + EPS)
                total = piece if total is None else total + piece
            cols = slice(p * LANES, (p + 1) * LANES)
            normed[q, :, cols] = (total * gain_ref[:, cols]).astype(BF)

    for q, to in ((far, far_id), (diag, diag_id), (near, near_id)):
        settle(q)
        h_copy(q, to).start()
    settle(t)

    wide_tile = 512 if width % 512 == 0 else width
    experts = lax.broadcasted_iota(jnp.int32, (max(n, 8), 1), 0)
    named_t = (routes_t_ref[0:1, :] == experts) | (routes_t_ref[1:2, :] == experts)
    row_r = lax.broadcasted_iota(jnp.int32, (rows, rows), 0)
    row_c = lax.broadcasted_iota(jnp.int32, (rows, rows), 1)
    named_t = named_t.astype(F32)
    ranks_t = jnp.dot(
        named_t.astype(BF), (row_r < row_c).astype(F32).astype(BF), preferred_element_type=F32
    )
    ranks_t = jnp.where(named_t > 0.0, ranks_t, -1.0)
    slots = lax.broadcasted_iota(jnp.int32, (cap, 1), 0).astype(F32)
    for e in range(n):
        into[e * cap : (e + 1) * cap, :] = jnp.where(
            ranks_t[e : e + 1, :] == slots, 1.0, 0.0
        ).astype(BF)
    first_e, second_e = routes_ref[:, 0:1], routes_ref[:, 1:2]
    named = ((first_e == lane) | (second_e == lane)).astype(F32)
    ranks = jnp.dot(
        (row_c < row_r).astype(F32).astype(BF), named.astype(BF), preferred_element_type=F32
    )
    wants = []
    for e in (first_e, second_e):
        rank = jnp.sum(jnp.where(e == lane, ranks, 0.0), axis=1, keepdims=True)
        wants.append(e.astype(F32) * cap + rank)
    wants = jnp.concatenate(wants, axis=0)

    wo_load.wait()
    resid_load.wait()

    def product(src, q, at):
        return jnp.dot(
            src,
            wo[pl.ds(pl.multiple_of(q * width_here, width_here), width_here), at : at + wide_tile],
            preferred_element_type=F32,
        )

    for at in range(0, width, wide_tile):
        wide[:, at : at + wide_tile] = product(normed[t], t, at)
    h_in(near).wait_recv()
    for at in range(0, width, wide_tile):
        wide[:, at : at + wide_tile] += product(gathered[near], near, at)
    h_in(far).wait_recv()
    h_in(diag).wait_recv()
    squares = jnp.zeros((rows, 1), F32)
    for at in range(0, width, wide_tile):
        cols = slice(at, at + wide_tile)
        value = (
            wide[:, cols]
            + product(gathered[far], far, at)
            + product(gathered[diag], diag, at)
            + resid[:, cols].astype(F32)
        )
        value = value.astype(BF).astype(F32)
        wide[:, cols] = value
        squares = squares + jnp.sum(value * value, axis=1, keepdims=True)
    scale = lax.rsqrt(squares / width + EPS)
    for at in range(0, width, wide_tile):
        cols = slice(at, at + wide_tile)
        xin[:, cols] = (wide[:, cols] * scale * norm_gain_ref[:, cols]).astype(BF)
    for at in range(0, width, wide_tile):
        cols = slice(at, at + wide_tile)
        sent = jnp.dot(into[...], xin[:, cols], preferred_element_type=F32).astype(BF)
        for e in range(n):
            out_ref[e, :, cols] = sent[e * cap : (e + 1) * cap]

    def source(k):
        return lax.rem(me - k + n, n)

    def a_out(k):
        to = lax.rem(me + k, n)
        return remote(
            out_ref.at[to], fan.at[me, t], a_send.at[k], a_recv.at[me], {"sp": to, "tp": t}
        )

    def a_in(k):
        p = source(k)
        return remote(out_ref.at[p], fan.at[p, t], a_send.at[k], a_recv.at[p], near_id)

    def x_copy(k, q):
        p = source(k)
        return remote(fan.at[p, q], fan.at[p, q], x_send.at[p], x_recv.at[p], far_id)

    def c_copy(k, q):
        p = source(k)
        return remote(fan.at[p, q], fan.at[p, q], c_send.at[p], c_recv.at[p], near_id)

    def d_copy(k, q):
        p = source(k)
        return remote(fan.at[p, q], fan.at[p, q], d_send.at[p], d_recv.at[p], near_id)

    def p_copy(k):
        p = source(k)
        return remote(part.at[p, 1 - c], got.at[p], p_send.at[p], p_recv.at[p], near_id)

    def s_copy(k):
        p = source(k)
        return remote(pair.at[p], across.at[p], s_send.at[p], s_recv.at[p], far_id)

    def r_out(k):
        p = source(k)
        return remote(fin.at[p], ret_ref.at[me], r_send.at[p], r_recv.at[me], {"sp": p, "tp": t})

    def r_in(k):
        p = source(k)
        return remote(fin.at[p], ret_ref.at[p], r_send.at[p], r_recv.at[p], near_id)

    own = pltpu.make_async_copy(out_ref.at[me], fan.at[me, t], own_sem)
    own.start()
    lax.fori_loop(1, n, lambda k, z_: (a_out(k).start(), z_)[1], 0)

    def spread(k):
        x_copy(k, t).start()
        c_copy(k, t).start()

    own.wait()
    spread(0)

    def step_a(k):
        a_in(k).wait_recv()
        spread(k)

    def step_x(k):
        x_copy(k, far).wait_recv()
        d_copy(k, far).start()

    def step_compute(k):
        p = source(k)
        c_copy(k, near).wait_recv()
        d_copy(k, diag).wait_recv()
        block = fan[p].reshape(4 * cap, width)
        gate = jnp.dot(block, wg[...], preferred_element_type=F32)
        up_ = jnp.dot(block, wu[...], preferred_element_type=F32)
        hidden[...] = (gate * jax.nn.sigmoid(gate) * up_).astype(BF)
        for at in range(0, width, wide_tile):
            down = jnp.dot(
                hidden[...], wd[:, at : at + wide_tile], preferred_element_type=F32
            ).astype(BF)
            for q in range(4):
                part[p, q % 2, q // 2, :, at : at + wide_tile] = down[q * cap : (q + 1) * cap]
        p_copy(k).start()

    def step_pair(k):
        p = source(k)
        p_copy(k).wait_recv()
        pair[p] = (part[p, c, 1 - xi].astype(F32) + got[p, 1 - xi].astype(F32)).astype(BF)
        s_copy(k).start()

    def step_final(k):
        p = source(k)
        s_copy(k).wait_recv()
        total = (
            part[p, c, xi].astype(F32) + got[p, xi].astype(F32) + across[p].astype(F32)
        ).astype(BF)

        @pl.when(k == 0)
        def _():
            ret_ref[me] = total

        @pl.when(k > 0)
        def _():
            fin[p] = total
            r_out(k).start()

    step_a(1)
    step_x(0)
    for copy in weights:
        copy.wait()

    def iteration(i, carry):
        @pl.when(i + 2 < n)
        def _():
            step_a(i + 2)

        @pl.when(i + 1 < n)
        def _():
            step_x(i + 1)

        @pl.when((i >= 1) & (i < n + 1))
        def _():
            step_pair(i - 1)

        @pl.when(i < n)
        def _():
            step_compute(i)

        @pl.when(i >= 2)
        def _():
            step_final(i - 2)

        return carry

    lax.fori_loop(0, n + 2, iteration, 0)

    slot = lax.broadcasted_iota(jnp.int32, (1, cap), 1)

    def combine(p):
        picks = (wants == (p * cap + slot).astype(F32)).astype(F32).astype(BF)
        for at in range(0, width, wide_tile):
            cols = slice(at, at + wide_tile)
            chosen = jnp.dot(picks, ret_ref[p, :, cols], preferred_element_type=F32)
            wide[:, cols] += (
                route_w_ref[:, 0:1] * chosen[:rows] + route_w_ref[:, 1:2] * chosen[rows:]
            )

    combine(me)

    def gather(i, carry):
        k = n - 1 - i
        r_in(k).wait_recv()
        combine(source(k))
        return carry

    lax.fori_loop(0, n - 1, gather, 0)
    mixed_ref[...] = wide[...].astype(BF)

    def sent_history(j, carry):
        d, i = j // chunks, lax.rem(j, chunks)

        @pl.when(rising(d))
        def _():
            up(d, i).wait_send()

        @pl.when(crossing(d))
        def _():
            over(d, i).wait_send()

        return carry

    lax.fori_loop(0, (reach + 1) * chunks, sent_history, 0)

    def sent_aux(k, carry):
        @pl.when(me + k < n)
        def _():
            aux_copy(k).wait_send()

        return carry

    lax.fori_loop(1, n // 2 + 1, sent_aux, 0)
    for q, to in ((far, far_id), (diag, diag_id), (near, near_id)):
        h_copy(q, to).wait_send()

    def finish(k, carry):
        x_copy(k, t).wait_send()
        c_copy(k, t).wait_send()
        d_copy(k, far).wait_send()
        p_copy(k).wait_send()
        s_copy(k).wait_send()

        @pl.when(k > 0)
        def _():
            a_out(k).wait_send()
            r_out(k).wait_send()

        return carry

    lax.fori_loop(0, n, finish, 0)


def on_device(
    queries,
    keys,
    values,
    cum_gate,
    documents,
    head_gain,
    out_weight,
    resid,
    norm_gain,
    routes,
    route_weights,
    w_gate,
    w_up,
    w_down,
):
    tokens, width_here = queries.shape
    heads_here = cum_gate.shape[1]
    head_size = width_here // heads_here
    n = lax.axis_size("sp")
    tp_count = lax.axis_size("tp")
    rows, width = resid.shape
    top_count = routes.shape[1]
    cap = 2 * top_count * tokens // (tp_count * n)
    hid = w_gate.shape[2]
    pairs, hpp = width_here // LANES, LANES // head_size
    part_len = tokens // SPLITS
    chunks = pairs * SPLITS
    reach = n // 4

    gates = cum_gate.T.reshape(pairs, hpp, SPLITS, part_len).transpose(0, 2, 1, 3)
    docs = jnp.broadcast_to(
        documents.astype(F32).reshape(1, SPLITS, 1, part_len), (pairs, SPLITS, 8 - hpp, part_len)
    )
    aux = jnp.concatenate([gates, docs], axis=2).reshape(chunks, 8, part_len)

    dma = pltpu.SemaphoreType.DMA
    hbm = pl.BlockSpec(memory_space=pl.ANY)
    vmem = pl.BlockSpec(memory_space=pltpu.VMEM)
    return pl.pallas_call(
        functools.partial(layer_kernel, n, head_size, cap),
        out_shape=jax.ShapeDtypeStruct((rows, width), BF),
        in_specs=[hbm] * 3 + [vmem] * 2 + [hbm] * 2 + [vmem] * 4 + [hbm] * 3,
        out_specs=vmem,
        scratch_shapes=[
            pltpu.VMEM((tokens, width_here), BF),
            pltpu.VMEM((pairs, hpp, tokens, LANES), BF),
            pltpu.VMEM((2 * reach + 2, chunks, 2, part_len, LANES), BF),
            pltpu.VMEM((n // 2 + 1, chunks, 8, part_len), F32),
            pltpu.VMEM((pairs, hpp, tokens, LANES), F32),
            pltpu.VMEM((pairs, hpp, tokens, LANES), F32),
            pltpu.VMEM((tp_count, rows, width_here), BF),
            pltpu.VMEM((tp_count, rows, width_here), BF),
            pltpu.VMEM((tp_count * width_here, width), BF),
            pltpu.VMEM((rows, width), BF),
            pltpu.VMEM((rows, width), F32),
            pltpu.VMEM((rows, width), BF),
            pltpu.VMEM((n * cap, rows), BF),
            pltpu.VMEM((n, cap, width), BF),
            pltpu.VMEM((n, cap, width), BF),
            pltpu.VMEM((n, 4, cap, width), BF),
            pltpu.VMEM((width, hid), BF),
            pltpu.VMEM((width, hid), BF),
            pltpu.VMEM((hid, width), BF),
            pltpu.VMEM((4 * cap, hid), BF),
            pltpu.VMEM((n, 2, 2, cap, width), BF),
            pltpu.VMEM((n, 2, cap, width), BF),
            pltpu.VMEM((n, cap, width), BF),
            pltpu.VMEM((n, cap, width), BF),
            pltpu.VMEM((n, cap, width), BF),
            dma((3,)),
            dma((2 * chunks,)),
            dma((3,)),
            dma,
        ]
        + [dma(((reach + 1) * chunks,)) for _ in range(4)]
        + [dma((n // 2 + 1,)) for _ in range(2)]
        + [dma((tp_count,)) for _ in range(2)]
        + [dma((n,)) for _ in range(14)],
        compiler_params=pltpu.CompilerParams(
            collective_id=1, has_side_effects=True, vmem_limit_bytes=VMEM_LIMIT
        ),
    )(
        queries,
        keys,
        values,
        aux,
        head_gain[None, :],
        out_weight,
        resid,
        norm_gain[None, :],
        routes,
        routes.T,
        route_weights,
        w_gate[0],
        w_up[0],
        w_down[0],
    )


def solution(mesh):
    in_specs = (
        P("sp", "tp"),
        P("sp", "tp"),
        P("sp", "tp"),
        P("sp", "tp"),
        P("sp"),
        P("tp"),
        P(),
        P(("sp", "tp"), None),
        P(),
        P(("sp", "tp"), None),
        P(("sp", "tp"), None),
        P("sp", None, "tp"),
        P("sp", None, "tp"),
        P("sp", "tp", None),
    )
    out_specs = P(("sp", "tp"), None)
    return jax.shard_map(
        on_device, mesh=mesh, in_specs=in_specs, out_specs=out_specs, check_vma=False
    )
```

profile of v0, /device:TPU:0, one launch (start us, length us, event | category | flops | bytes accessed | tf_op | source)
XLA Modules:
  0.0 187.9 jit_solution(1188725966262507277)
XLA Ops:
  0.0 0.7 convert_element_type.3
  0.7 0.7 reshape.8
  1.4 0.6 pad_maximum_fusion
  2.0 1.4 copy.17.route_w_ref
  3.4 1.4 copy.16.routes_ref
  4.9 181.1 %shard_map.136 = bf16[128,2048]{1,0:T(8,128)(2,1)} custom-call(bf16[512,256]{1,0:T(8,128)(2,1)} %q_hbm.1, bf16[512,256]{1,0:T(8,128)(2,1)} %k_hbm.1, bf16[512,256]{1,0:T(8,128)(2,1)} %v_hbm.1, f32[4,8,256]{2,1,0:T(8,128)} %bitcast.14, f32[1,256]{1,0:T(1,128)} %bitcast.19, bf16[1024,2048]{1,0:T(8,128)(2,1)} %wo_hbm.1, bf16[128,2048]{1,0:T(8,128)(2,1)} %resid_hbm.1, ...), custom_call_target="tpu_custom_call" | custom-call | tf_op jit(solution)/shard_map/pallas_call | solution.py:649
  186.0 1.9 %copy.21 = bf16[128,2048]{1,0:T(8,128)(2,1)} copy(bf16[128,2048]{1,0:T(8,128)(2,1)} %shard_map.136) | data formatting | bytes 1048576
  (3 shorter events, 0.0 us)
where the time goes:
time: 188 us
  Pallas kernels  181 us (96%)
  local copies, waits for them, and re-layouts  5.44 us (3%)
    pallas_call x1, Pallas kernels, on_device(): pl.pallas_call(functools.partial(layer_kernel, n, head_size, cap), out_sh...  181 us
    unnamed x3, local copies, waits for them, and re-layouts  4.7 us

commit v1 on v0

--- a/solution.py
+++ b/solution.py
@@ -10,7 +10,7 @@
 EPS = 1e-06
 MESH = pl.DeviceIdType.MESH
 NEG = -1e30
-VMEM_LIMIT = 65000 * 1024
+VMEM_LIMIT = 67043328
 LANES = 128
 SPLITS = 2
 BF = jnp.bfloat16
@@ -24,13 +24,13 @@
     q_hbm,
     k_hbm,
     v_hbm,
-    aux_ref,
+    gates_ref,
+    docs_ref,
     gain_ref,
     wo_hbm,
     resid_hbm,
     norm_gain_ref,
     routes_ref,
-    routes_t_ref,
     route_w_ref,
     wg_hbm,
     wu_hbm,
@@ -39,17 +39,18 @@
     q_in,
     qs,
     kv,
+    aux_ref,
     aux_all,
+    route_own,
+    route_all,
     top,
     acc,
     normed,
     gathered,
     wo,
-    resid,
     wide,
-    xin,
-    into,
-    out_ref,
+    raw,
+    crossing_rows,
     ret_ref,
     fan,
     wg,
@@ -58,13 +59,10 @@
     hidden,
     part,
     got,
-    pair,
     across,
-    fin,
     in_sem,
     kv_sem,
     w_sem,
-    own_sem,
     up_send,
     up_recv,
     over_send,
@@ -73,8 +71,13 @@
     aux_recv,
     h_send,
     h_recv,
-    a_send,
-    a_recv,
+    route_send,
+    route_recv,
+    rise_send,
+    fall_send,
+    raw_recv,
+    y_send,
+    y_recv,
     x_send,
     x_recv,
     c_send,
@@ -101,6 +104,7 @@
     diag_id = {"sp": me, "tp": diag}
     mate_id = {"sp": me + 1 - 2 * y, "tp": t}
     above_id = {"sp": lax.rem(me + 2, n), "tp": t}
+    below_id = {"sp": lax.rem(me + n - 2, n), "tp": t}
 
     tokens, width_here = q_in.shape
     pairs = width_here // LANES
@@ -121,7 +125,7 @@
     ]
     q_load = pltpu.make_async_copy(q_hbm, q_in, in_sem.at[0])
     wo_load = pltpu.make_async_copy(wo_hbm, wo, in_sem.at[1])
-    resid_load = pltpu.make_async_copy(resid_hbm, resid, in_sem.at[2])
+    resid_load = pltpu.make_async_copy(resid_hbm, raw.at[z], in_sem.at[2])
     weights = [
         pltpu.make_async_copy(src, dst, w_sem.at[i])
         for i, (src, dst) in enumerate(((wg_hbm, wg), (wu_hbm, wu), (wd_hbm, wd)))
@@ -130,6 +134,15 @@
         copy.start()
     q_load.start()
 
+    for p in range(pairs):
+        for s in range(SPLITS):
+            cols = slice(s * keys, (s + 1) * keys)
+            doc_row = docs_ref[:, cols].astype(F32)
+            aux_ref[p * SPLITS + s] = jnp.concatenate(
+                [gates_ref[p * hpp : (p + 1) * hpp, cols]] + [doc_row] * (8 - hpp), axis=0
+            )
+    route_own[...] = jnp.concatenate([routes_ref[...]] * 4, axis=0)
+
     barrier = pltpu.get_barrier_semaphore()
 
     def greet(k, carry):
@@ -208,6 +221,27 @@
         return carry
 
     lax.fori_loop(1, n // 2 + 1, send_aux, 0)
+
+    def route_copy(b):
+        return remote(
+            route_own,
+            route_all.at[z],
+            route_send.at[b],
+            route_recv.at[z],
+            {"sp": 2 * b + y, "tp": t},
+        )
+
+    def route_in(b):
+        return remote(route_own, route_all.at[b], route_send.at[b], route_recv.at[b], near_id)
+
+    def send_route(b, carry):
+        @pl.when(b != z)
+        def _():
+            route_copy(b).start()
+
+        return carry
+
+    lax.fori_loop(0, floors, send_route, 0)
     wo_load.start()
     resid_load.start()
     for copy in weights:
@@ -318,10 +352,14 @@
             aux_here(2 * d, i)
             earlier(d, 2 * d, i)
 
-        crossed(d - 1, i)
+        @pl.when(d >= 2)
+        def _():
+            crossed(d - 2, i)
+
         return carry
 
     lax.fori_loop(0, reach * chunks, history, 0)
+    lax.fori_loop(0, chunks, lambda i, z_: (crossed(reach - 1, i), z_)[1], 0)
     lax.fori_loop(0, chunks, lambda i, z_: (crossed(reach, i), z_)[1], 0)
 
     def h_copy(q, to):
@@ -350,30 +388,33 @@
     settle(t)
 
     wide_tile = 512 if width % 512 == 0 else width
-    experts = lax.broadcasted_iota(jnp.int32, (max(n, 8), 1), 0)
-    named_t = (routes_t_ref[0:1, :] == experts) | (routes_t_ref[1:2, :] == experts)
     row_r = lax.broadcasted_iota(jnp.int32, (rows, rows), 0)
     row_c = lax.broadcasted_iota(jnp.int32, (rows, rows), 1)
-    named_t = named_t.astype(F32)
-    ranks_t = jnp.dot(
-        named_t.astype(BF), (row_r < row_c).astype(F32).astype(BF), preferred_element_type=F32
-    )
-    ranks_t = jnp.where(named_t > 0.0, ranks_t, -1.0)
+
+    def column(row):
+        return jnp.sum(jnp.where(row_r == row_c, row, 0.0), axis=1, keepdims=True)
+
+    before_row = (row_r < row_c).astype(F32).astype(BF)
     slots = lax.broadcasted_iota(jnp.int32, (cap, 1), 0).astype(F32)
-    for e in range(n):
-        into[e * cap : (e + 1) * cap, :] = jnp.where(
-            ranks_t[e : e + 1, :] == slots, 1.0, 0.0
-        ).astype(BF)
-    first_e, second_e = routes_ref[:, 0:1], routes_ref[:, 1:2]
-    named = ((first_e == lane) | (second_e == lane)).astype(F32)
+
+    def taken(routes, e):
+        named = ((routes[0:1, :] == e) | (routes[1:2, :] == e)).astype(F32)
+        spread_out = jnp.broadcast_to(named, (8, rows)).astype(BF)
+        rank = jnp.dot(spread_out, before_row, preferred_element_type=F32)[0:1]
+        return ((named > 0.0) & (rank == slots)).astype(F32).astype(BF)
+
+    first_e, second_e = [column(routes_ref[r : r + 1, :].astype(F32)) for r in range(2)]
+    lane_f = lane.astype(F32)
+    named = ((first_e == lane_f) | (second_e == lane_f)).astype(F32)
     ranks = jnp.dot(
         (row_c < row_r).astype(F32).astype(BF), named.astype(BF), preferred_element_type=F32
     )
     wants = []
     for e in (first_e, second_e):
-        rank = jnp.sum(jnp.where(e == lane, ranks, 0.0), axis=1, keepdims=True)
-        wants.append(e.astype(F32) * cap + rank)
+        rank = jnp.sum(jnp.where(e == lane_f, ranks, 0.0), axis=1, keepdims=True)
+        wants.append(e * cap + rank)
     wants = jnp.concatenate(wants, axis=0)
+    route_weights = [column(route_w_ref[r : r + 1, :]) for r in range(2)]
 
     wo_load.wait()
     resid_load.wait()
@@ -399,33 +440,88 @@
             wide[:, cols]
             + product(gathered[far], far, at)
             + product(gathered[diag], diag, at)
-            + resid[:, cols].astype(F32)
+            + raw[z, :, cols].astype(F32)
         )
         value = value.astype(BF).astype(F32)
         wide[:, cols] = value
         squares = squares + jnp.sum(value * value, axis=1, keepdims=True)
     scale = lax.rsqrt(squares / width + EPS)
-    for at in range(0, width, wide_tile):
-        cols = slice(at, at + wide_tile)
-        xin[:, cols] = (wide[:, cols] * scale * norm_gain_ref[:, cols]).astype(BF)
-    for at in range(0, width, wide_tile):
-        cols = slice(at, at + wide_tile)
-        sent = jnp.dot(into[...], xin[:, cols], preferred_element_type=F32).astype(BF)
-        for e in range(n):
-            out_ref[e, :, cols] = sent[e * cap : (e + 1) * cap]
+    halves = 2
+    half = width // halves
+
+    def raw_part(b, h):
+        return raw.at[b, :, pl.ds(h * half, half)]
+
+    def carry_raw(b, h, send, to):
+        return remote(
+            raw_part(b, h), raw_part(b, h), send.at[b * halves + h], raw_recv.at[b * halves + h], to
+        )
+
+    def rise(b, h):
+        return carry_raw(b, h, rise_send, above_id)
+
+    def fall(b, h):
+        return carry_raw(b, h, fall_send, below_id)
+
+    for h in range(halves):
+        for at in range(h * half, (h + 1) * half, min(wide_tile, half)):
+            cols = slice(at, at + min(wide_tile, half))
+            raw[z, :, cols] = (wide[:, cols] * scale * norm_gain_ref[:, cols]).astype(BF)
+
+        @pl.when(z + 1 < floors)
+        def _():
+            rise(z, h).start()
+
+        @pl.when(z > 0)
+        def _():
+            fall(z, h).start()
+
+    def floor_at(j):
+        return jnp.where(j <= z, z - j, j)
 
     def source(k):
-        return lax.rem(me - k + n, n)
-
-    def a_out(k):
-        to = lax.rem(me + k, n)
+        return 2 * floor_at(k // 2) + jnp.where(lax.rem(k, 2) == 0, y, 1 - y)
+
+    def arrive(j):
+        below, above = z - j, z + j
+
+        @pl.when(below >= 0)
+        def _():
+            for h in range(halves):
+                rise(below, h).wait_recv()
+
+                @pl.when(z + 1 < floors)
+                def _():
+                    rise(below, h).start()
+
+        @pl.when(above < floors)
+        def _():
+            for h in range(halves):
+                fall(above, h).wait_recv()
+
+                @pl.when(z > 0)
+                def _():
+                    fall(above, h).start()
+
+    def y_copy(b):
         return remote(
-            out_ref.at[to], fan.at[me, t], a_send.at[k], a_recv.at[me], {"sp": to, "tp": t}
-        )
-
-    def a_in(k):
-        p = source(k)
-        return remote(out_ref.at[p], fan.at[p, t], a_send.at[k], a_recv.at[p], near_id)
+            crossing_rows.at[b], fan.at[2 * b + y, t], y_send.at[b], y_recv.at[b], mate_id
+        )
+
+    def y_in(b):
+        return remote(
+            crossing_rows.at[b], fan.at[2 * b + 1 - y, t], y_send.at[b], y_recv.at[b], mate_id
+        )
+
+    def select(b, routes):
+        mate = me + 1 - 2 * y
+        picks = jnp.concatenate([taken(routes, mate), taken(routes, me)], axis=0)
+        for at in range(0, width, wide_tile):
+            cols = slice(at, at + wide_tile)
+            both = jnp.dot(picks, raw[b, :, cols], preferred_element_type=F32).astype(BF)
+            crossing_rows[b, :, cols] = both[:cap]
+            fan[2 * b + y, t, :, cols] = both[cap:]
+        y_copy(b).start()
 
     def x_copy(k, q):
         p = source(k)
@@ -445,29 +541,34 @@
 
     def s_copy(k):
         p = source(k)
-        return remote(pair.at[p], across.at[p], s_send.at[p], s_recv.at[p], far_id)
+        return remote(part.at[p, c, 1 - xi], across.at[p], s_send.at[p], s_recv.at[p], far_id)
 
     def r_out(k):
         p = source(k)
-        return remote(fin.at[p], ret_ref.at[me], r_send.at[p], r_recv.at[me], {"sp": p, "tp": t})
-
-    def r_in(k):
-        p = source(k)
-        return remote(fin.at[p], ret_ref.at[p], r_send.at[p], r_recv.at[p], near_id)
-
-    own = pltpu.make_async_copy(out_ref.at[me], fan.at[me, t], own_sem)
-    own.start()
-    lax.fori_loop(1, n, lambda k, z_: (a_out(k).start(), z_)[1], 0)
+        return remote(
+            part.at[p, c, xi], ret_ref.at[me], r_send.at[p], r_recv.at[me], {"sp": p, "tp": t}
+        )
+
+    def r_in(p):
+        return remote(part.at[p, c, xi], ret_ref.at[p], r_send.at[p], r_recv.at[p], near_id)
 
     def spread(k):
         x_copy(k, t).start()
         c_copy(k, t).start()
 
-    own.wait()
-    spread(0)
-
     def step_a(k):
-        a_in(k).wait_recv()
+        j = k // 2
+
+        @pl.when(lax.rem(k, 2) == 0)
+        def _():
+            arrive(j)
+            route_in(floor_at(j)).wait_recv()
+            select(floor_at(j), route_all[floor_at(j)])
+
+        @pl.when(lax.rem(k, 2) == 1)
+        def _():
+            y_in(floor_at(j)).wait_recv()
+
         spread(k)
 
     def step_x(k):
@@ -493,7 +594,9 @@
     def step_pair(k):
         p = source(k)
         p_copy(k).wait_recv()
-        pair[p] = (part[p, c, 1 - xi].astype(F32) + got[p, 1 - xi].astype(F32)).astype(BF)
+        part[p, c, 1 - xi] = (
+            part[p, c, 1 - xi].astype(F32) + got[p, 1 - xi].astype(F32)
+        ).astype(BF)
         s_copy(k).start()
 
     def step_final(k):
@@ -509,9 +612,11 @@
 
         @pl.when(k > 0)
         def _():
-            fin[p] = total
+            part[p, c, xi] = total
             r_out(k).start()
 
+    select(z, routes_ref[...])
+    spread(0)
     step_a(1)
     step_x(0)
     for copy in weights:
@@ -550,18 +655,18 @@
             cols = slice(at, at + wide_tile)
             chosen = jnp.dot(picks, ret_ref[p, :, cols], preferred_element_type=F32)
             wide[:, cols] += (
-                route_w_ref[:, 0:1] * chosen[:rows] + route_w_ref[:, 1:2] * chosen[rows:]
+                route_weights[0] * chosen[:rows] + route_weights[1] * chosen[rows:]
             )
 
     combine(me)
 
     def gather(i, carry):
-        k = n - 1 - i
-        r_in(k).wait_recv()
-        combine(source(k))
-        return carry
-
-    lax.fori_loop(0, n - 1, gather, 0)
+        p = source(i)
+        r_in(p).wait_recv()
+        combine(p)
+        return carry
+
+    lax.fori_loop(1, n, gather, 0)
     mixed_ref[...] = wide[...].astype(BF)
 
     def sent_history(j, carry):
@@ -589,6 +694,26 @@
     lax.fori_loop(1, n // 2 + 1, sent_aux, 0)
     for q, to in ((far, far_id), (diag, diag_id), (near, near_id)):
         h_copy(q, to).wait_send()
+
+    def sent_floor(b, carry):
+        y_copy(b).wait_send()
+
+        @pl.when(b != z)
+        def _():
+            route_copy(b).wait_send()
+
+        for h in range(halves):
+            @pl.when((b <= z) & (z + 1 < floors))
+            def _():
+                rise(b, h).wait_send()
+
+            @pl.when((b >= z) & (z > 0))
+            def _():
+                fall(b, h).wait_send()
+
+        return carry
+
+    lax.fori_loop(0, floors, sent_floor, 0)
 
     def finish(k, carry):
         x_copy(k, t).wait_send()
@@ -599,7 +724,6 @@
 
         @pl.when(k > 0)
         def _():
-            a_out(k).wait_send()
             r_out(k).wait_send()
 
         return carry
@@ -637,35 +761,30 @@
     chunks = pairs * SPLITS
     reach = n // 4
 
-    gates = cum_gate.T.reshape(pairs, hpp, SPLITS, part_len).transpose(0, 2, 1, 3)
-    docs = jnp.broadcast_to(
-        documents.astype(F32).reshape(1, SPLITS, 1, part_len), (pairs, SPLITS, 8 - hpp, part_len)
-    )
-    aux = jnp.concatenate([gates, docs], axis=2).reshape(chunks, 8, part_len)
-
     dma = pltpu.SemaphoreType.DMA
     hbm = pl.BlockSpec(memory_space=pl.ANY)
     vmem = pl.BlockSpec(memory_space=pltpu.VMEM)
     return pl.pallas_call(
         functools.partial(layer_kernel, n, head_size, cap),
         out_shape=jax.ShapeDtypeStruct((rows, width), BF),
-        in_specs=[hbm] * 3 + [vmem] * 2 + [hbm] * 2 + [vmem] * 4 + [hbm] * 3,
+        in_specs=[hbm] * 3 + [vmem] * 3 + [hbm] * 2 + [vmem] * 3 + [hbm] * 3,
         out_specs=vmem,
         scratch_shapes=[
             pltpu.VMEM((tokens, width_here), BF),
             pltpu.VMEM((pairs, hpp, tokens, LANES), BF),
             pltpu.VMEM((2 * reach + 2, chunks, 2, part_len, LANES), BF),
+            pltpu.VMEM((chunks, 8, part_len), F32),
             pltpu.VMEM((n // 2 + 1, chunks, 8, part_len), F32),
+            pltpu.VMEM((8, rows), jnp.int32),
+            pltpu.VMEM((n // 2, 8, rows), jnp.int32),
             pltpu.VMEM((pairs, hpp, tokens, LANES), F32),
             pltpu.VMEM((pairs, hpp, tokens, LANES), F32),
             pltpu.VMEM((tp_count, rows, width_here), BF),
             pltpu.VMEM((tp_count, rows, width_here), BF),
             pltpu.VMEM((tp_count * width_here, width), BF),
-            pltpu.VMEM((rows, width), BF),
             pltpu.VMEM((rows, width), F32),
-            pltpu.VMEM((rows, width), BF),
-            pltpu.VMEM((n * cap, rows), BF),
-            pltpu.VMEM((n, cap, width), BF),
+            pltpu.VMEM((n // 2, rows, width), BF),
+            pltpu.VMEM((n // 2, cap, width), BF),
             pltpu.VMEM((n, cap, width), BF),
             pltpu.VMEM((n, 4, cap, width), BF),
             pltpu.VMEM((width, hid), BF),
@@ -675,17 +794,17 @@
             pltpu.VMEM((n, 2, 2, cap, width), BF),
             pltpu.VMEM((n, 2, cap, width), BF),
             pltpu.VMEM((n, cap, width), BF),
-            pltpu.VMEM((n, cap, width), BF),
-            pltpu.VMEM((n, cap, width), BF),
             dma((3,)),
             dma((2 * chunks,)),
             dma((3,)),
-            dma,
         ]
         + [dma(((reach + 1) * chunks,)) for _ in range(4)]
         + [dma((n // 2 + 1,)) for _ in range(2)]
         + [dma((tp_count,)) for _ in range(2)]
-        + [dma((n,)) for _ in range(14)],
+        + [dma((n // 2,)) for _ in range(2)]
+        + [dma((n,)) for _ in range(3)]
+        + [dma((n // 2,)) for _ in range(2)]
+        + [dma((n,)) for _ in range(12)],
         compiler_params=pltpu.CompilerParams(
             collective_id=1, has_side_effects=True, vmem_limit_bytes=VMEM_LIMIT
         ),
@@ -693,14 +812,14 @@
         queries,
         keys,
         values,
-        aux,
+        cum_gate.T,
+        documents[None, :],
         head_gain[None, :],
         out_weight,
         resid,
         norm_gain[None, :],
-        routes,
         routes.T,
-        route_weights,
+        route_weights.T,
         w_gate[0],
         w_up[0],
         w_down[0],

time: 188 us -> 169 us (0.90)
  Pallas kernels: 181 us -> 167 us
  local copies, waits for them, and re-layouts: 5.44 us -> 1.88 us
    pallas_call x1, Pallas kernels: 181 us -> 167 us  [on_device(): pl.pallas_call(functools.partial(layer_kernel, n, head_size, cap), out_sh...]
    unnamed x3 -> x1, local copies, waits for them, and re-layouts: 4.7 us -> 1.88 us
where the time goes in v1:
time: 169 us
  Pallas kernels  167 us (99%)
  local copies, waits for them, and re-layouts  1.88 us (1%)
    pallas_call x1, Pallas kernels, on_device(): pl.pallas_call(functools.partial(layer_kernel, n, head_size, cap), out_sh...  167 us

profile of v1, /device:TPU:0, one launch (start us, length us, event | category | flops | bytes accessed | tf_op | source)
XLA Modules:
  0.0 169.2 jit_solution(8484389015986287458)
XLA Ops:
  0.0 167.3 %shard_map.136 = bf16[128,2048]{1,0:T(8,128)(2,1)} custom-call(bf16[512,256]{1,0:T(8,128)(2,1)} %q_hbm.1, bf16[512,256]{1,0:T(8,128)(2,1)} %k_hbm.1, bf16[512,256]{1,0:T(8,128)(2,1)} %v_hbm.1, f32[4,512]{1,0:T(4,128)} %bitcast.12, s32[1,512]{1,0:T(1,128)} %bitcast.14, f32[1,256]{1,0:T(1,128)} %bitcast.15, bf16[1024,2048]{1,0:T(8,128)(2,1)} %wo_hbm.1, ...), custom_call_target="tpu_custom_call" | custom-call | tf_op jit(solution)/shard_map/pallas_call | solution.py:767
  167.3 1.9 %copy.16 = bf16[128,2048]{1,0:T(8,128)(2,1)} copy(bf16[128,2048]{1,0:T(8,128)(2,1)} %shard_map.136) | data formatting | bytes 1048576

commit v2 on v1

--- a/solution.py
+++ b/solution.py
@@ -134,13 +134,13 @@
         copy.start()
     q_load.start()
 
-    for p in range(pairs):
-        for s in range(SPLITS):
-            cols = slice(s * keys, (s + 1) * keys)
-            doc_row = docs_ref[:, cols].astype(F32)
-            aux_ref[p * SPLITS + s] = jnp.concatenate(
-                [gates_ref[p * hpp : (p + 1) * hpp, cols]] + [doc_row] * (8 - hpp), axis=0
-            )
+    heads = pairs * hpp
+    for s in range(SPLITS):
+        cols = slice(s * keys, (s + 1) * keys)
+        doc_row = docs_ref[:, cols].astype(F32)
+        aux_ref[s] = jnp.concatenate(
+            [gates_ref[:, cols]] + [doc_row] * (aux_ref.shape[1] - heads), axis=0
+        )
     route_own[...] = jnp.concatenate([routes_ref[...]] * 4, axis=0)
 
     barrier = pltpu.get_barrier_semaphore()
@@ -208,19 +208,19 @@
         def _():
             over(d, i).start()
 
+    pl.semaphore_wait(barrier, n + 2)
+
+    def send_aux(k, carry):
+        @pl.when(me + k < n)
+        def _():
+            aux_copy(k).start()
+
+        return carry
+
+    lax.fori_loop(1, n // 2 + 1, send_aux, 0)
     for copy in loads:
         copy.wait()
-    pl.semaphore_wait(barrier, n + 2)
     lax.fori_loop(0, chunks, lambda i, z_: (forward(0, i), z_)[1], 0)
-
-    def send_aux(k, carry):
-        @pl.when(me + k < n)
-        def _():
-            aux_copy(k).start()
-
-        return carry
-
-    lax.fori_loop(1, n // 2 + 1, send_aux, 0)
 
     def route_copy(b):
         return remote(
@@ -283,12 +283,12 @@
             exps.astype(BF), v, preferred_element_type=F32
         )
 
-    first_doc = aux_ref[0][hpp : hpp + 1, 0:1]
+    first_doc = aux_ref[0, heads : heads + 1, 0:1]
     spots_r = lax.broadcasted_iota(jnp.int32, (keys, keys), 0)
     spots_c = lax.broadcasted_iota(jnp.int32, (keys, keys), 1)
     doc_cols = [
         jnp.sum(
-            jnp.where(spots_r == spots_c, aux_ref[s][hpp : hpp + 1, :], 0.0), axis=1, keepdims=True
+            jnp.where(spots_r == spots_c, aux_ref[s, heads : heads + 1, :], 0.0), axis=1, keepdims=True
         )
         for s in range(SPLITS)
     ]
@@ -297,17 +297,17 @@
     def diagonal(p, carry):
         for s in range(SPLITS):
             i = p * SPLITS + s
-            side = aux_ref[i]
+            docs_here = aux_ref[s, heads : heads + 1, :]
             for h in range(hpp):
-                base = aux_ref[p * SPLITS][h : h + 1, 0:1]
-                bias = base - side[h : h + 1, :]
+                gate_at = pl.ds(p * hpp + h, 1)
+                bias = aux_ref[0, gate_at, :][:, 0:1] - aux_ref[s, gate_at, :]
                 for r0 in range(0, tokens, tile):
                     if r0 + tile <= s * keys:
                         continue
                     key_pos = s * keys + lax.broadcasted_iota(jnp.int32, (1, keys), 1)
                     query_pos = r0 + lax.broadcasted_iota(jnp.int32, (tile, 1), 0)
                     allowed = (key_pos <= query_pos) & (
-                        side[hpp : hpp + 1, :] == doc_col[r0 : r0 + tile]
+                        docs_here == doc_col[r0 : r0 + tile]
                     )
                     visit(0, i, p, h, r0, bias, allowed)
         return carry
@@ -319,12 +319,12 @@
             top[p, h] = jnp.where(shut > 0.0, 1e30, top[p, h])
 
     def earlier(slot, dist, i):
-        p = i // SPLITS
-        side = aux_all[dist, i]
-        zero = aux_ref[p * SPLITS]
+        p, s = i // SPLITS, lax.rem(i, SPLITS)
+        same = aux_all[dist, s, heads : heads + 1, :] == first_doc
         for h in range(hpp):
+            gate_at = pl.ds(p * hpp + h, 1)
             bias = jnp.where(
-                side[hpp : hpp + 1, :] == first_doc, zero[h : h + 1, 0:1] - side[h : h + 1, :], NEG
+                same, aux_ref[0, gate_at, :][:, 0:1] - aux_all[dist, s, gate_at, :], NEG
             )
             for r0 in range(0, tokens, tile):
                 visit(slot, i, p, h, r0, bias, None)
@@ -476,14 +476,19 @@
         def _():
             fall(z, h).start()
 
+    both_ways = jnp.minimum(z, floors - 1 - z)
+
     def floor_at(j):
-        return jnp.where(j <= z, z - j, j)
+        step = jnp.where(j <= 2 * both_ways, (j + 1) // 2, j - both_ways)
+        down = jnp.where(j <= 2 * both_ways, lax.rem(j, 2) == 1, 2 * z >= floors)
+        return jnp.where(down, z - step, z + step)
 
     def source(k):
         return 2 * floor_at(k // 2) + jnp.where(lax.rem(k, 2) == 0, y, 1 - y)
 
     def arrive(j):
-        below, above = z - j, z + j
+        later = jnp.where(z > 0, j - 1, j)
+        below, above = z - j, z + later
 
         @pl.when(below >= 0)
         def _():
@@ -494,7 +499,7 @@
                 def _():
                     rise(below, h).start()
 
-        @pl.when(above < floors)
+        @pl.when((above < floors) & (later > 0))
         def _():
             for h in range(halves):
                 fall(above, h).wait_recv()
@@ -618,34 +623,40 @@
     select(z, routes_ref[...])
     spread(0)
     step_a(1)
-    step_x(0)
+    for k in (2, 3):
+        step_a(k)
     for copy in weights:
         copy.wait()
 
+    def turn(i):
+        return jnp.where(i + 2 < n, i + 2, n - 1 - i)
+
+    step_x(turn(0))
+
     def iteration(i, carry):
-        @pl.when(i + 2 < n)
-        def _():
-            step_a(i + 2)
+        @pl.when(i + 4 < n)
+        def _():
+            step_a(i + 4)
 
         @pl.when(i + 1 < n)
         def _():
-            step_x(i + 1)
-
-        @pl.when((i >= 1) & (i < n + 1))
-        def _():
-            step_pair(i - 1)
+            step_x(turn(i + 1))
+
+        @pl.when(i >= 1)
+        def _():
+            step_pair(turn(i - 1))
 
         @pl.when(i < n)
         def _():
-            step_compute(i)
+            step_compute(turn(i))
 
         @pl.when(i >= 2)
         def _():
-            step_final(i - 2)
-
-        return carry
-
-    lax.fori_loop(0, n + 2, iteration, 0)
+            step_final(turn(i - 2))
+
+        return carry
+
+    lax.fori_loop(0, n + 1, iteration, 0)
 
     slot = lax.broadcasted_iota(jnp.int32, (1, cap), 1)
 
@@ -658,15 +669,16 @@
                 route_weights[0] * chosen[:rows] + route_weights[1] * chosen[rows:]
             )
 
-    combine(me)
-
     def gather(i, carry):
-        p = source(i)
+        p = source(turn(i))
         r_in(p).wait_recv()
         combine(p)
         return carry
 
-    lax.fori_loop(1, n, gather, 0)
+    lax.fori_loop(0, n - 2, gather, 0)
+    step_final(0)
+    combine(me)
+    gather(n - 2, 0)
     mixed_ref[...] = wide[...].astype(BF)
 
     def sent_history(j, carry):
@@ -760,6 +772,7 @@
     part_len = tokens // SPLITS
     chunks = pairs * SPLITS
     reach = n // 4
+    side_rows = -(-(heads_here + 1) // 8) * 8
 
     dma = pltpu.SemaphoreType.DMA
     hbm = pl.BlockSpec(memory_space=pl.ANY)
@@ -773,8 +786,8 @@
             pltpu.VMEM((tokens, width_here), BF),
             pltpu.VMEM((pairs, hpp, tokens, LANES), BF),
             pltpu.VMEM((2 * reach + 2, chunks, 2, part_len, LANES), BF),
-            pltpu.VMEM((chunks, 8, part_len), F32),
-            pltpu.VMEM((n // 2 + 1, chunks, 8, part_len), F32),
+            pltpu.VMEM((SPLITS, side_rows, part_len), F32),
+            pltpu.VMEM((n // 2 + 1, SPLITS, side_rows, part_len), F32),
             pltpu.VMEM((8, rows), jnp.int32),
             pltpu.VMEM((n // 2, 8, rows), jnp.int32),
             pltpu.VMEM((pairs, hpp, tokens, LANES), F32),

time: 169 us -> 157 us (0.929)
  Pallas kernels: 167 us -> 155 us
    pallas_call x1, Pallas kernels: 167 us -> 155 us  [on_device(): pl.pallas_call(functools.partial(layer_kernel, n, head_size, cap), out_sh...]
where the time goes in v2:
time: 157 us
  Pallas kernels  155 us (99%)
  local copies, waits for them, and re-layouts  1.88 us (1%)
    pallas_call x1, Pallas kernels, on_device(): pl.pallas_call(functools.partial(layer_kernel, n, head_size, cap), out_sh...  155 us

profile of v2, /device:TPU:0, one launch (start us, length us, event | category | flops | bytes accessed | tf_op | source)
XLA Modules:
  0.0 157.1 jit_solution(14849121115101137509)
XLA Ops:
  0.0 155.2 %shard_map.136 = bf16[128,2048]{1,0:T(8,128)(2,1)} custom-call(bf16[512,256]{1,0:T(8,128)(2,1)} %q_hbm.1, bf16[512,256]{1,0:T(8,128)(2,1)} %k_hbm.1, bf16[512,256]{1,0:T(8,128)(2,1)} %v_hbm.1, f32[4,512]{1,0:T(4,128)} %bitcast.12, s32[1,512]{1,0:T(1,128)} %bitcast.14, f32[1,256]{1,0:T(1,128)} %bitcast.15, bf16[1024,2048]{1,0:T(8,128)(2,1)} %wo_hbm.1, ...), custom_call_target="tpu_custom_call" | custom-call | tf_op jit(solution)/shard_map/pallas_call | solution.py:780
  155.2 1.9 %copy.16 = bf16[128,2048]{1,0:T(8,128)(2,1)} copy(bf16[128,2048]{1,0:T(8,128)(2,1)} %shard_map.136) | data formatting | bytes 1048576

commit v3 on v2

--- a/solution.py
+++ b/solution.py
@@ -35,6 +35,7 @@
     wg_hbm,
     wu_hbm,
     wd_hbm,
+    mixed_hbm,
     mixed_ref,
     q_in,
     qs,
@@ -358,6 +359,35 @@
 
         return carry
 
+    wide_tile = 512 if width % 512 == 0 else width
+    row_r = lax.broadcasted_iota(jnp.int32, (rows, rows), 0)
+    row_c = lax.broadcasted_iota(jnp.int32, (rows, rows), 1)
+
+    def column(row):
+        return jnp.sum(jnp.where(row_r == row_c, row, 0.0), axis=1, keepdims=True)
+
+    before_row = (row_r < row_c).astype(F32).astype(BF)
+    slots = lax.broadcasted_iota(jnp.int32, (cap, 1), 0).astype(F32)
+
+    def taken(routes, e):
+        named = ((routes[0:1, :] == e) | (routes[1:2, :] == e)).astype(F32)
+        spread_out = jnp.broadcast_to(named, (8, rows)).astype(BF)
+        rank = jnp.dot(spread_out, before_row, preferred_element_type=F32)[0:1]
+        return ((named > 0.0) & (rank == slots)).astype(F32).astype(BF)
+
+    first_e, second_e = [column(routes_ref[r : r + 1, :].astype(F32)) for r in range(2)]
+    lane_f = lane.astype(F32)
+    named = ((first_e == lane_f) | (second_e == lane_f)).astype(F32)
+    ranks = jnp.dot(
+        (row_c < row_r).astype(F32).astype(BF), named.astype(BF), preferred_element_type=F32
+    )
+    wants = []
+    for e in (first_e, second_e):
+        rank = jnp.sum(jnp.where(e == lane_f, ranks, 0.0), axis=1, keepdims=True)
+        wants.append(e * cap + rank)
+    wants = jnp.concatenate(wants, axis=0)
+    route_weights = [column(route_w_ref[r : r + 1, :]) for r in range(2)]
+
     lax.fori_loop(0, reach * chunks, history, 0)
     lax.fori_loop(0, chunks, lambda i, z_: (crossed(reach - 1, i), z_)[1], 0)
     lax.fori_loop(0, chunks, lambda i, z_: (crossed(reach, i), z_)[1], 0)
@@ -386,35 +416,6 @@
         settle(q)
         h_copy(q, to).start()
     settle(t)
-
-    wide_tile = 512 if width % 512 == 0 else width
-    row_r = lax.broadcasted_iota(jnp.int32, (rows, rows), 0)
-    row_c = lax.broadcasted_iota(jnp.int32, (rows, rows), 1)
-
-    def column(row):
-        return jnp.sum(jnp.where(row_r == row_c, row, 0.0), axis=1, keepdims=True)
-
-    before_row = (row_r < row_c).astype(F32).astype(BF)
-    slots = lax.broadcasted_iota(jnp.int32, (cap, 1), 0).astype(F32)
-
-    def taken(routes, e):
-        named = ((routes[0:1, :] == e) | (routes[1:2, :] == e)).astype(F32)
-        spread_out = jnp.broadcast_to(named, (8, rows)).astype(BF)
-        rank = jnp.dot(spread_out, before_row, preferred_element_type=F32)[0:1]
-        return ((named > 0.0) & (rank == slots)).astype(F32).astype(BF)
-
-    first_e, second_e = [column(routes_ref[r : r + 1, :].astype(F32)) for r in range(2)]
-    lane_f = lane.astype(F32)
-    named = ((first_e == lane_f) | (second_e == lane_f)).astype(F32)
-    ranks = jnp.dot(
-        (row_c < row_r).astype(F32).astype(BF), named.astype(BF), preferred_element_type=F32
-    )
-    wants = []
-    for e in (first_e, second_e):
-        rank = jnp.sum(jnp.where(e == lane_f, ranks, 0.0), axis=1, keepdims=True)
-        wants.append(e * cap + rank)
-    wants = jnp.concatenate(wants, axis=0)
-    route_weights = [column(route_w_ref[r : r + 1, :]) for r in range(2)]
 
     wo_load.wait()
     resid_load.wait()
@@ -463,6 +464,31 @@
     def fall(b, h):
         return carry_raw(b, h, fall_send, below_id)
 
+    def bring(b):
+        @pl.when(b < z)
+        def _():
+            for h in range(halves):
+                rise(b, h).wait_recv()
+
+                @pl.when(z + 1 < floors)
+                def _():
+                    rise(b, h).start()
+
+        @pl.when(b > z)
+        def _():
+            for h in range(halves):
+                fall(b, h).wait_recv()
+
+                @pl.when(z > 0)
+                def _():
+                    fall(b, h).start()
+
+    inner = (z > 0) & (z + 1 < floors)
+
+    @pl.when((z == 1) & inner)
+    def _():
+        bring(0)
+
     for h in range(halves):
         for at in range(h * half, (h + 1) * half, min(wide_tile, half)):
             cols = slice(at, at + min(wide_tile, half))
@@ -476,37 +502,21 @@
         def _():
             fall(z, h).start()
 
-    both_ways = jnp.minimum(z, floors - 1 - z)
+    over_here = floors - 1 - z
+    both_ways = jnp.maximum(jnp.minimum(z - 1, over_here), 0)
 
     def floor_at(j):
-        step = jnp.where(j <= 2 * both_ways, (j + 1) // 2, j - both_ways)
-        down = jnp.where(j <= 2 * both_ways, lax.rem(j, 2) == 1, 2 * z >= floors)
-        return jnp.where(down, z - step, z + step)
+        turns = j - 1
+        paired = turns <= 2 * both_ways
+        step = jnp.where(paired, (turns + 1) // 2, turns - both_ways)
+        up_next = jnp.where(paired, lax.rem(turns, 2) == 1, over_here > z - 1)
+        mid = jnp.where(j == 1, 0, jnp.where(up_next, z + step, z - step))
+        last = jnp.where(j == 1, z - 1, jnp.where(j == 2, 0, z + 1 - j))
+        at = jnp.where(z == 0, j, jnp.where(over_here == 0, last, mid))
+        return jnp.where(j == 0, z, at)
 
     def source(k):
         return 2 * floor_at(k // 2) + jnp.where(lax.rem(k, 2) == 0, y, 1 - y)
-
-    def arrive(j):
-        later = jnp.where(z > 0, j - 1, j)
-        below, above = z - j, z + later
-
-        @pl.when(below >= 0)
-        def _():
-            for h in range(halves):
-                rise(below, h).wait_recv()
-
-                @pl.when(z + 1 < floors)
-                def _():
-                    rise(below, h).start()
-
-        @pl.when((above < floors) & (later > 0))
-        def _():
-            for h in range(halves):
-                fall(above, h).wait_recv()
-
-                @pl.when(z > 0)
-                def _():
-                    fall(above, h).start()
 
     def y_copy(b):
         return remote(
@@ -566,12 +576,24 @@
 
         @pl.when(lax.rem(k, 2) == 0)
         def _():
-            arrive(j)
+
+            @pl.when(jnp.logical_not(inner))
+            def _():
+                bring(floor_at(j))
+
+            @pl.when(inner & (j <= z) & (z > 1))
+            def _():
+                bring(jnp.where(j == 1, 0, z + 1 - j))
+
             route_in(floor_at(j)).wait_recv()
             select(floor_at(j), route_all[floor_at(j)])
 
         @pl.when(lax.rem(k, 2) == 1)
         def _():
+            @pl.when(inner & (j >= 1) & (z + j < floors))
+            def _():
+                bring(z + j)
+
             y_in(floor_at(j)).wait_recv()
 
         spread(k)
@@ -680,6 +702,8 @@
     combine(me)
     gather(n - 2, 0)
     mixed_ref[...] = wide[...].astype(BF)
+    leave = pltpu.make_async_copy(mixed_ref, mixed_hbm, in_sem.at[0])
+    leave.start()
 
     def sent_history(j, carry):
         d, i = j // chunks, lax.rem(j, chunks)
@@ -741,6 +765,7 @@
         return carry
 
     lax.fori_loop(0, n, finish, 0)
+    leave.wait()
 
 
 def on_device(
@@ -781,8 +806,9 @@
         functools.partial(layer_kernel, n, head_size, cap),
         out_shape=jax.ShapeDtypeStruct((rows, width), BF),
         in_specs=[hbm] * 3 + [vmem] * 3 + [hbm] * 2 + [vmem] * 3 + [hbm] * 3,
-        out_specs=vmem,
+        out_specs=hbm,
         scratch_shapes=[
+            pltpu.VMEM((rows, width), BF),
             pltpu.VMEM((tokens, width_here), BF),
             pltpu.VMEM((pairs, hpp, tokens, LANES), BF),
             pltpu.VMEM((2 * reach + 2, chunks, 2, part_len, LANES), BF),

time: 157 us -> 156 us (level)
  the two profiles are of different devices: /device:TPU:0 before, /device:TPU:30 now
where the time goes in v3:
time: 156 us; the launch traced here: 155 us
  Pallas kernels  153 us (98%)
  local copies, waits for them, and re-layouts  1.88 us (1%)
    pallas_call x1, Pallas kernels, on_device(): pl.pallas_call(functools.partial(layer_kernel, n, head_size, cap), out_sh...  153 us

profile of v3, /device:TPU:30, one launch (start us, length us, event | category | flops | bytes accessed | tf_op | source)
XLA Modules:
  0.0 155.4 jit_solution(3281569532344799311)
XLA Ops:
  0.0 153.5 %shard_map.136 = bf16[128,2048]{1,0:T(8,128)(2,1)} custom-call(bf16[512,256]{1,0:T(8,128)(2,1)} %q_hbm.1, bf16[512,256]{1,0:T(8,128)(2,1)} %k_hbm.1, bf16[512,256]{1,0:T(8,128)(2,1)} %v_hbm.1, f32[4,512]{1,0:T(4,128)} %bitcast.12, s32[1,512]{1,0:T(1,128)} %bitcast.14, f32[1,256]{1,0:T(1,128)} %bitcast.15, bf16[1024,2048]{1,0:T(8,128)(2,1)} %wo_hbm.1, ...), custom_call_target="tpu_custom_call" | custom-call | tf_op jit(solution)/shard_map/pallas_call | solution.py:805
  153.5 1.9 %copy.16 = bf16[128,2048]{1,0:T(8,128)(2,1)} copy(bf16[128,2048]{1,0:T(8,128)(2,1)} %shard_map.136) | data formatting | bytes 1048576
